TPU v7x, 32 devices: a whole 2x2x4 slice. The times are simulated.
32 devices in a mesh: ep: 8 (over z, core), tp: 4 (over y, x).
Axes of the slice: x: 2, y: 2, z: 4, core: 2. Of those that a mesh axis runs over, the one named last changes fastest.
Arguments:
- tokens: bfloat16 [2048, 2048], P('ep', 'tp'), may hold values from -800 to 800
- norm_gain: bfloat16 [2048], P('tp'), may hold values from 0.099609375 to 1.8984375
- w_gate: bfloat16 [8, 2048, 6144], P('ep', None, 'tp'), may hold values from -0.125 to 0.125
- w_up: bfloat16 [8, 2048, 6144], P('ep', None, 'tp'), may hold values from -0.125 to 0.125
- w_down: bfloat16 [8, 6144, 2048], P('ep', 'tp'), may hold values from -1.2757759 to 1.2757759
- routes: int32 [2048, 2], P('ep'), may hold values from 0 to 7, all different within a row; in each aligned block of 256 rows (0 to 255, 256 to 511, ...) at most 128 rows name the same one
- route_weights: float32 [2048, 2], P('ep'), may hold values from 0.1 to 1
- final_gain: bfloat16 [2048], P('tp'), may hold values from 0.099609375 to 1.8984375
Outputs:
- mixed_out: bfloat16 [2048, 2048], P('ep', 'tp')
Inputs may be any that keep to these rules, and one draw needn't show every extreme that they name: `routes`: A token's 2 experts differ. Among the tokens of one index of ep (aligned blocks of 256 rows), no expert is named by more than 128 tokens, a bound that some block reaches.
All inputs are finite; a program needn't handle non-finite values.
Results may differ from a plain program's by a relative error of at most 0.017.
Values may be sent and summed in bfloat16 or wider, within the bound.
A program may use at most 64 MiB of HBM per device.

v0:
```python
import jax
import jax.numpy as jnp
from jax import lax
from jax.sharding import PartitionSpec as P

EPS = 1e-06


def slot_targets(routes, experts, capacity):
    flat = routes.reshape(-1)
    onehot = (flat[:, None] == jnp.arange(experts, dtype=jnp.int32)[None, :]).astype(jnp.int32)
    before = jnp.cumsum(onehot, axis=0) - onehot
    slot = jnp.sum(before * onehot, axis=1)
    return flat * capacity + slot


def local(tokens, norm_gain, w_gate, w_up, w_down, routes, route_weights, final_gain):
    experts = lax.axis_size("ep")
    tok_rows = tokens.shape[0]
    share = tokens.shape[1]
    width = share * lax.axis_size("tp")
    topk = routes.shape[1]
    capacity = 2 * tok_rows * topk // experts
    wide = tokens.astype(jnp.float32)
    input_squares = lax.psum(jnp.sum(wide * wide, axis=1), "tp")
    scale = lax.rsqrt(input_squares / width + EPS)
    normed = (wide * scale[:, None] * norm_gain.astype(jnp.float32)[None, :]).astype(jnp.bfloat16)
    target = slot_targets(routes, experts, capacity)
    sources = jnp.repeat(jnp.arange(tok_rows, dtype=jnp.int32), topk)
    gate_w = w_gate[0]
    up_w = w_up[0]
    down_w = w_down[0]
    outbox = jnp.zeros((experts * capacity, share), jnp.bfloat16).at[target].set(normed[sources])
    inbox = lax.all_to_all(outbox, "ep", split_axis=0, concat_axis=0, tiled=True)
    piece = lax.all_gather(inbox, "tp", axis=1, tiled=True)
    gate = jnp.dot(piece, gate_w, preferred_element_type=jnp.float32)
    up = jnp.dot(piece, up_w, preferred_element_type=jnp.float32)
    hidden = (jax.nn.silu(gate) * up).astype(jnp.bfloat16)
    sums = lax.psum_scatter(
        lax.dot_general(
            down_w, hidden, (((0,), (1,)), ((), ())), preferred_element_type=jnp.float32
        ).astype(jnp.bfloat16),
        "tp",
        scatter_dimension=0,
        tiled=True,
    )
    returned = lax.all_to_all(sums, "ep", split_axis=1, concat_axis=1, tiled=True)
    picked = jnp.take(returned, target, axis=1).reshape(returned.shape[0], tok_rows, topk)
    combined = jnp.einsum("dtk,tk->td", picked.astype(jnp.float32), route_weights)
    local_squares = jnp.sum(combined * combined, axis=1)
    total_squares = lax.psum(local_squares, "tp")
    final_scale = lax.rsqrt(total_squares / width + EPS)
    return (combined * final_scale[:, None] * final_gain.astype(jnp.float32)[None, :]).astype(
        jnp.bfloat16
    )


def solution(mesh):
    in_specs = (
        P("ep", "tp"),
        P("tp"),
        P("ep", None, "tp"),
        P("ep", None, "tp"),
        P("ep", "tp", None),
        P("ep", None),
        P("ep", None),
        P("tp"),
    )
    out_specs = P("ep", "tp")
    return jax.shard_map(local, mesh=mesh, in_specs=in_specs, out_specs=out_specs, check_vma=False)
```

profile of v0, /device:TPU:0, one launch (start us, length us, event | category | flops | bytes accessed | tf_op | source)
XLA Modules:
  0.0 247.3 jit_solution(9177944375881044333)
XLA Ops:
  6.5 0.8 copy.13
  7.6 0.7 broadcast_multiply_fusion
  8.3 1.1 reduce-window.6
  9.5 0.2 slice_reduce_fusion
  10.0 1.1 fusion.12
  11.1 11.4 %psum.14 = f32[256]{0:T(256)S(1)} all-reduce(f32[256]{0:T(256)S(1)} %fusion.12), channel_id=1, replica_groups=mesh['ep'=8,'tp'=4] {'tp'}, use_global_device_ids=true, to_apply=%region_4.5 | all-reduce | flops 256 | bytes 2048 | tf_op jit(solution)/shard_map/psum | solution.py:25
  22.5 0.7 convert_element_type.35
  23.5 1.1 fusion.14
  24.5 5.0 %scatter_custom_fusion = bf16[1024,512]{1,0:T(8,128)(2,1)S(1)} fusion(s32[512]{0:T(512)S(1)} %bitcast.54, bf16[256,512]{1,0:T(8,128)(2,1)S(1)} %fusion.14, s32[1024]{0:T(1024)S(1)} %pad_clamp_fusion.1, bf16[]{:T(256)} %constant.18.clone.1), kind=kCustom, calls=%fused_computation.22 | custom fusion | bytes 1048578 | tf_op jit(solution)/shard_map/scatter | solution.py:33
  29.6 31.3 %all_to_all.24 = bf16[8,128,512]{2,1,0:T(8,128)(2,1)} all-to-all(bf16[8,128,512]{2,1,0:T(8,128)(2,1)S(1)} %bitcast.50), channel_id=1, replica_groups=mesh['ep'=8,'tp'=4] {'ep'}, dimensions={0} | all-to-all | bytes 2097152 | tf_op jit(solution)/shard_map/all_to_all | solution.py:34
  61.0 0.2 reduce-scatter.2.cloned.1.call-start
  61.2 49.4 %all-gather.2.cloned.1.call-done = bf16[1024,2048]{1,0:T(8,128)(2,1)} async-done(((bf16[1024,512]{1,0:T(8,128)(2,1)}), bf16[1024,2048]{1,0:T(8,128)(2,1)}) %all-gather.2.cloned.1.call-update) | async-done | bytes 4194320 | tf_op jit(solution)/shard_map/all_gather | solution.py:35
  110.6 11.7 %fusion.4 = f32[1024,1536]{1,0:T(8,128)} fusion(bf16[1024,2048]{1,0:T(8,128)(2,1)} %all-gather.2.cloned.1.call-done, bf16[1,2048,1536]{2,1,0:T(8,128)(2,1)} %param.10), kind=kOutput, calls=%fused_computation.7 | convolution fusion | flops 6442450944 | bytes 16777216 | tf_op jit(solution)/shard_map/dot_general | solution.py:36
  122.3 21.0 %convert_bitcast_fusion = bf16[2048,1024]{0,1:T(8,128)(2,1)} fusion(bf16[1,1536,2048]{2,1,0:T(8,128)(2,1)} %param.12, f32[1024,1536]{1,0:T(8,128)} %fusion.4, bf16[1024,2048]{1,0:T(8,128)(2,1)} %all-gather.2.cloned.1.call-done, bf16[1,2048,1536]{2,1,0:T(8,128)(2,1)} %param.11), kind=kOutput, calls=%fused_computation.10 | convolution fusion | flops 12896436224 | bytes 27262976 | tf_op jit(solution)/shard_map/dot_general | solution.py:40
  143.4 52.7 %reduce-scatter.2.cloned.1.call-done = bf16[512,1024]{0,1:T(8,128)(2,1)} async-done(((bf16[2048,1024]{0,1:T(8,128)(2,1)}), bf16[512,1024]{0,1:T(8,128)(2,1)}) %reduce-scatter.2.cloned.1.call-update) | async-done | bytes 1048592 | tf_op jit(solution)/shard_map/reduce_scatter | solution.py:39
  196.1 4.6 %all-to-all-start.1 = ((bf16[512,8,128]{0,2,1:T(8,128)(2,1)}), bf16[512,8,128]{0,2,1:T(8,128)(2,1)S(1)}, u32[]{:S(2)}, u32[]{:S(2)}) async-start(bf16[512,8,128]{0,2,1:T(8,128)(2,1)} %bitcast.52), calls=%async_computation.2 | async-start | bytes 2097152 | tf_op jit(solution)/shard_map/all_to_all | solution.py:47
  201.0 0.2 copy.16
  201.1 0.2 copy.18
  201.4 25.9 %all-to-all-done.1 = bf16[512,8,128]{0,2,1:T(8,128)(2,1)S(1)} async-done(((bf16[512,8,128]{0,2,1:T(8,128)(2,1)}), bf16[512,8,128]{0,2,1:T(8,128)(2,1)S(1)}, u32[]{:S(2)}, u32[]{:S(2)}) %all-to-all-start.1) | async-done | bytes 1048608 | tf_op jit(solution)/shard_map/all_to_all | solution.py:47
  227.3 2.0 gather_fusion
  229.2 0.2 gather.11
  229.5 1.1 fusion.21
  230.6 9.0 %psum.15 = f32[256]{0:T(256)S(1)} all-reduce(f32[256]{0:T(256)S(1)} %fusion.15), channel_id=1, replica_groups=mesh['ep'=8,'tp'=4] {'tp'}, use_global_device_ids=true, to_apply=%region_8.9 | all-reduce | flops 256 | bytes 2048 | tf_op jit(solution)/shard_map/psum | solution.py:51
  239.6 0.8 fusion.17
  (30 shorter events, 1.3 us)
Async XLA Ops:
  6.5 104.1 %all-gather.2.cloned.1.call-start = ((), (), s32[]{:S(2)}) async-start(), calls=%async_computation.3 | async-start | bytes 5242880 | tf_op jit(solution)/shard_map/all_gather | solution.py:35
  61.0 135.1 %reduce-scatter.2.cloned.1.call-start = ((), (), s32[]{:S(2)}) async-start(), calls=%async_computation.4 | async-start | bytes 5242880 | tf_op jit(solution)/shard_map/reduce_scatter | solution.py:39
  143.3 57.6 %copy-start = (s32[256,2]{0,1:T(2,128)S(1)}, s32[256,2]{0,1:T(2,128)}, u32[]{:S(2)}) copy-start(s32[256,2]{0,1:T(2,128)} %param.13) | copy-start | bytes 6148
  143.3 57.8 %copy-start.1 = (f32[256,2]{0,1:T(2,128)S(1)}, f32[256,2]{0,1:T(2,128)}, u32[]{:S(2)}) copy-start(f32[256,2]{0,1:T(2,128)} %param.14) | copy-start | bytes 6148
  143.3 58.0 %copy-start.2 = (bf16[512]{0:T(512)(128)(2,1)S(1)}, bf16[512]{0:T(512)(128)(2,1)}, u32[]{:S(2)}) copy-start(bf16[512]{0:T(512)(128)(2,1)} %param.15) | copy-start | bytes 3076
  196.1 31.2 %all-to-all-start.1 = ((bf16[512,8,128]{0,2,1:T(8,128)(2,1)}), bf16[512,8,128]{0,2,1:T(8,128)(2,1)S(1)}, u32[]{:S(2)}, u32[]{:S(2)}) async-start(bf16[512,8,128]{0,2,1:T(8,128)(2,1)} %bitcast.52), calls=%async_computation.2 | async-start | bytes 2097152 | tf_op jit(solution)/shard_map/all_to_all | solution.py:47
Sparse Core Ops, SparseCore 0:
  61.1 49.4 all-gather.1
  143.5 52.5 reduce-scatter.1
where the time goes:
time: 248 us; the launch traced here: 247 us
  waiting for transfers between devices  128 us (52%)
  blocking collectives  51.7 us (21%)
  matrix products  33.8 us (14%)
  between operations  13.6 us (5%)
  local copies, waits for them, and re-layouts  9.53 us (4%)
  other arithmetic  5.79 us (2%)
  starting transfers between devices  4.83 us (2%)
    reduce_scatter x1, waiting for transfers between devices, local(): lax.psum_scatter(lax.dot_general(down_w, hidden, (((0,), (1,)), ((), ()))...  52.7 us
    all_gather x1, waiting for transfers between devices, local(): piece = lax.all_gather(inbox, 'tp', axis=1, tiled=True)  49.4 us
    all_to_all x1, blocking collectives, local(): lax.all_to_all(outbox, 'ep', split_axis=0, concat_axis=0, tiled=True)  31.3 us
    all_to_all x1, waiting for transfers between devices, local(): lax.all_to_all(sums, 'ep', split_axis=1, concat_axis=1, tiled=True)  25.9 us
    dot_general x1, matrix products, local(): lax.dot_general(down_w, hidden, (((0,), (1,)), ((), ())), preferred_eleme...  21 us
    dot_general x1, matrix products, local(): gate = jnp.dot(piece, gate_w, preferred_element_type=jnp.float32)  11.7 us
    psum x1, blocking collectives, local(): input_squares = lax.psum(jnp.sum(wide * wide, axis=1), 'tp')  11.4 us
    psum x1, blocking collectives, local(): total_squares = lax.psum(local_squares, 'tp')  8.95 us
  transfers between devices with their start and end apart: 3, of which 3 were waited for; matrix products, arithmetic and copies ran while one was open for 0% of the time, Pallas kernels for 0%

commit v1 on v0

--- a/solution.py
+++ b/solution.py
@@ -44,7 +44,9 @@
         scatter_dimension=0,
         tiled=True,
     )
-    returned = lax.all_to_all(sums, "ep", split_axis=1, concat_axis=1, tiled=True)
+    returned = jnp.concatenate(
+        lax.all_to_all(jnp.stack(jnp.split(sums, lax.axis_size("ep"), axis=1)), "ep", 0, 0), axis=1
+    )
     picked = jnp.take(returned, target, axis=1).reshape(returned.shape[0], tok_rows, topk)
     combined = jnp.einsum("dtk,tk->td", picked.astype(jnp.float32), route_weights)
     local_squares = jnp.sum(combined * combined, axis=1)

time: 248 us -> 260 us (1.048)
  local copies, waits for them, and re-layouts: 9.53 us -> 22 us
    unnamed x8 -> x15, local copies, waits for them, and re-layouts: 0.99 us -> 11.9 us
where the time goes in v1:
time: 260 us
  waiting for transfers between devices  128 us (49%)
  blocking collectives  51.7 us (20%)
  matrix products  33.8 us (13%)
  local copies, waits for them, and re-layouts  22 us (8%)
  between operations  13.6 us (5%)
  other arithmetic  5.79 us (2%)
  starting transfers between devices  4.83 us (2%)
    reduce_scatter x1, waiting for transfers between devices, local(): lax.psum_scatter(lax.dot_general(down_w, hidden, (((0,), (1,)), ((), ()))...  52.7 us
    all_gather x1, waiting for transfers between devices, local(): piece = lax.all_gather(inbox, 'tp', axis=1, tiled=True)  49.4 us
    all_to_all x1, blocking collectives, local(): lax.all_to_all(outbox, 'ep', split_axis=0, concat_axis=0, tiled=True)  31.3 us
    all_to_all x1, waiting for transfers between devices, local(): lax.all_to_all(jnp.stack(jnp.split(sums, lax.axis_size('ep'), axis=1)), '...  25.9 us
    dot_general x1, matrix products, local(): lax.dot_general(down_w, hidden, (((0,), (1,)), ((), ())), preferred_eleme...  21 us
    unnamed x15, local copies, waits for them, and re-layouts  11.9 us
    dot_general x1, matrix products, local(): gate = jnp.dot(piece, gate_w, preferred_element_type=jnp.float32)  11.7 us
    psum x1, blocking collectives, local(): input_squares = lax.psum(jnp.sum(wide * wide, axis=1), 'tp')  11.4 us
  transfers between devices with their start and end apart: 3, of which 3 were waited for; matrix products, arithmetic and copies ran while one was open for 0% of the time, Pallas kernels for 0%

profile of v1, /device:TPU:0, one launch (start us, length us, event | category | flops | bytes accessed | tf_op | source)
XLA Modules:
  0.0 259.7 jit_solution(5530802697532318886)
XLA Ops:
  8.3 1.1 reduce-window.6
  10.0 1.1 fusion.12
  11.1 11.4 %psum.14 = f32[256]{0:T(256)S(1)} all-reduce(f32[256]{0:T(256)S(1)} %fusion.12), channel_id=1, replica_groups=mesh['ep'=8,'tp'=4] {'tp'}, use_global_device_ids=true, to_apply=%region_4.5 | all-reduce | flops 256 | bytes 2048 | tf_op jit(solution)/shard_map/psum | solution.py:25
  23.5 1.1 fusion.14
  24.5 5.0 %scatter_custom_fusion = bf16[1024,512]{1,0:T(8,128)(2,1)S(1)} fusion(s32[512]{0:T(512)S(1)} %bitcast.86, bf16[256,512]{1,0:T(8,128)(2,1)S(1)} %fusion.14, s32[1024]{0:T(1024)S(1)} %pad_clamp_fusion.1, bf16[]{:T(256)} %constant.18.clone.1), kind=kCustom, calls=%fused_computation.22 | custom fusion | bytes 1048578 | tf_op jit(solution)/shard_map/scatter | solution.py:33
  29.6 31.3 %all_to_all.17 = bf16[8,128,512]{2,1,0:T(8,128)(2,1)} all-to-all(bf16[8,128,512]{2,1,0:T(8,128)(2,1)S(1)} %bitcast.83), channel_id=1, replica_groups=mesh['ep'=8,'tp'=4] {'ep'}, dimensions={0} | all-to-all | bytes 2097152 | tf_op jit(solution)/shard_map/all_to_all | solution.py:34
  61.2 49.4 %all-gather.2.cloned.1.call-done = bf16[1024,2048]{1,0:T(8,128)(2,1)} async-done(((bf16[1024,512]{1,0:T(8,128)(2,1)}), bf16[1024,2048]{1,0:T(8,128)(2,1)}) %all-gather.2.cloned.1.call-update) | async-done | bytes 4194320 | tf_op jit(solution)/shard_map/all_gather | solution.py:35
  110.6 11.7 %fusion.4 = f32[1024,1536]{1,0:T(8,128)} fusion(bf16[1024,2048]{1,0:T(8,128)(2,1)} %all-gather.2.cloned.1.call-done, bf16[1,2048,1536]{2,1,0:T(8,128)(2,1)} %param.10), kind=kOutput, calls=%fused_computation.7 | convolution fusion | flops 6442450944 | bytes 16777216 | tf_op jit(solution)/shard_map/dot_general | solution.py:36
  122.3 21.0 %convert_bitcast_fusion = bf16[2048,1024]{0,1:T(8,128)(2,1)} fusion(bf16[1,1536,2048]{2,1,0:T(8,128)(2,1)} %param.12, f32[1024,1536]{1,0:T(8,128)} %fusion.4, bf16[1024,2048]{1,0:T(8,128)(2,1)} %all-gather.2.cloned.1.call-done, bf16[1,2048,1536]{2,1,0:T(8,128)(2,1)} %param.11), kind=kOutput, calls=%fused_computation.10 | convolution fusion | flops 12896436224 | bytes 27262976 | tf_op jit(solution)/shard_map/dot_general | solution.py:40
  143.4 52.7 %reduce-scatter.2.cloned.1.call-done = bf16[512,1024]{0,1:T(8,128)(2,1)} async-done(((bf16[2048,1024]{0,1:T(8,128)(2,1)}), bf16[512,1024]{0,1:T(8,128)(2,1)}) %reduce-scatter.2.cloned.1.call-update) | async-done | bytes 1048592 | tf_op jit(solution)/shard_map/reduce_scatter | solution.py:39
  196.1 1.6 fusion.30
  197.7 1.6 fusion.29
  199.2 1.6 fusion.28
  200.8 1.6 fusion.27
  202.3 1.6 fusion.26
  203.9 1.6 fusion.25
  205.5 1.6 fusion.24
  207.0 1.6 fusion.23
  208.6 4.6 %all-to-all-start.1 = ((bf16[8,512,128]{1,2,0:T(8,128)(2,1)}), bf16[8,512,128]{1,2,0:T(8,128)(2,1)S(1)}, u32[]{:S(2)}, u32[]{:S(2)}) async-start(bf16[8,512,128]{1,2,0:T(8,128)(2,1)} %fusion.23), calls=%async_computation.2 | async-start | bytes 2097152 | tf_op jit(solution)/shard_map/all_to_all | solution.py:48
  213.8 25.9 %all-to-all-done.1 = bf16[8,512,128]{1,2,0:T(8,128)(2,1)S(1)} async-done(((bf16[8,512,128]{1,2,0:T(8,128)(2,1)}), bf16[8,512,128]{1,2,0:T(8,128)(2,1)S(1)}, u32[]{:S(2)}, u32[]{:S(2)}) %all-to-all-start.1) | async-done | bytes 1048608 | tf_op jit(solution)/shard_map/all_to_all | solution.py:48
  239.8 2.0 gather_fusion
  241.9 1.1 fusion.21
  243.1 9.0 %psum.15 = f32[256]{0:T(256)S(1)} all-reduce(f32[256]{0:T(256)S(1)} %fusion.15), channel_id=1, replica_groups=mesh['ep'=8,'tp'=4] {'tp'}, use_global_device_ids=true, to_apply=%region_8.9 | all-reduce | flops 256 | bytes 2048 | tf_op jit(solution)/shard_map/psum | solution.py:53
  252.1 0.8 fusion.17
  (38 shorter events, 4.5 us)
Async XLA Ops:
  6.5 104.1 %all-gather.2.cloned.1.call-start = ((), (), s32[]{:S(2)}) async-start(), calls=%async_computation.3 | async-start | bytes 5242880 | tf_op jit(solution)/shard_map/all_gather | solution.py:35
  61.0 135.1 %reduce-scatter.2.cloned.1.call-start = ((), (), s32[]{:S(2)}) async-start(), calls=%async_computation.4 | async-start | bytes 5242880 | tf_op jit(solution)/shard_map/reduce_scatter | solution.py:39
  143.3 70.1 %copy-start = (s32[256,2]{0,1:T(2,128)S(1)}, s32[256,2]{0,1:T(2,128)}, u32[]{:S(2)}) copy-start(s32[256,2]{0,1:T(2,128)} %param.13) | copy-start | bytes 6148
  143.3 70.3 %copy-start.1 = (f32[256,2]{0,1:T(2,128)S(1)}, f32[256,2]{0,1:T(2,128)}, u32[]{:S(2)}) copy-start(f32[256,2]{0,1:T(2,128)} %param.14) | copy-start | bytes 6148
  143.3 70.5 %copy-start.2 = (bf16[512]{0:T(512)(128)(2,1)S(1)}, bf16[512]{0:T(512)(128)(2,1)}, u32[]{:S(2)}) copy-start(bf16[512]{0:T(512)(128)(2,1)} %param.15) | copy-start | bytes 3076
  208.6 31.2 %all-to-all-start.1 = ((bf16[8,512,128]{1,2,0:T(8,128)(2,1)}), bf16[8,512,128]{1,2,0:T(8,128)(2,1)S(1)}, u32[]{:S(2)}, u32[]{:S(2)}) async-start(bf16[8,512,128]{1,2,0:T(8,128)(2,1)} %fusion.23), calls=%async_computation.2 | async-start | bytes 2097152 | tf_op jit(solution)/shard_map/all_to_all | solution.py:48
Sparse Core Ops, SparseCore 0:
  61.1 49.4 all-gather.1
  143.5 52.5 reduce-scatter.1
